TPU v7x, 32 devices: a whole 2x2x4 slice. The times are simulated.
32 devices in a mesh: sp: 4 (over x, core), tp: 8 (over z, y).
Axes of the slice: x: 2, y: 2, z: 4, core: 2. Of those that a mesh axis runs over, the one named last changes fastest.
Arguments:
- latents: bfloat16 [1024, 2048], P(('sp', 'tp')), may hold values from -6 to 6
- context: bfloat16 [256, 2048], P('sp'), may hold values from -6 to 6
- condition: float32 [2048], P('sp'), may hold values from -12 to 12
- context_condition: float32 [2048], P('sp'), may hold values from -12 to 12
- norm_gain: float32 [2048], replicated, may hold values from 0.1 to 1.9
- shift_weight: bfloat16 [2048, 2048], P('sp', 'tp'), may hold values from -0.09375 to 0.09375
- scale_weight: bfloat16 [2048, 2048], P('sp', 'tp'), may hold values from -0.09375 to 0.09375
- gate_weight: bfloat16 [2048, 2048], P('sp', 'tp'), may hold values from -0.125 to 0.125
- query_weight: bfloat16 [2048, 1024], P(None, 'tp'), may hold values from -0.125 to 0.125
- key_weight: bfloat16 [2048, 1024], P(None, 'tp'), may hold values from -0.125 to 0.125
- value_weight: bfloat16 [2048, 1024], P(None, 'tp'), may hold values from -0.125 to 0.125
- subtract_share: float32 [8], P('tp'), may hold values from 0.3 to 0.8
- head_gain: float32 [128], replicated, may hold values from 0.1 to 1.9
- output_weight: bfloat16 [1024, 2048], P('tp'), may hold values from -0.1875 to 0.1875
Outputs:
- updated: bfloat16 [1024, 2048], P(('sp', 'tp'))
All inputs are finite; a program needn't handle non-finite values.
Results may differ from a plain program's by a relative error of at most 0.013.
Values may be sent and summed in bfloat16 or wider, within the bound.
A program may use at most 64 MiB of HBM per device.

v0:
```python
import jax
import jax.numpy as jnp
from jax import lax
from jax.sharding import PartitionSpec as P

HEAD = 64
VALUE = 128
GRID_W = 64
norm_eps = 1e-06
head_eps = 1e-05
rope_theta = 10000.0
head_scale = 0.8


def rotary_tables(positions):
    quarter = HEAD // 4
    inverse = rope_theta ** (-2.0 * jnp.arange(quarter, dtype=jnp.float32) / (HEAD // 2))
    row_angle = (positions // GRID_W).astype(jnp.float32)[:, None] * inverse[None, :]
    column_angle = (positions % GRID_W).astype(jnp.float32)[:, None] * inverse[None, :]
    angles = jnp.concatenate([row_angle, row_angle, column_angle, column_angle], axis=-1)
    return (jnp.cos(angles), jnp.sin(angles))


def rotate(vectors, cosine, sine_table):
    quarter = HEAD // 4
    pieces = vectors.reshape(vectors.shape[:-1] + (2, 2, quarter))
    turned = jnp.concatenate([-pieces[..., 1:, :], pieces[..., :1, :]], axis=-2).reshape(
        vectors.shape
    )
    return vectors * cosine[:, None, :] + turned * sine_table[:, None, :]


def modulate(token_rows, gain_row, shift_row, scale_row):
    widened = token_rows.astype(jnp.float32)
    normed = widened * lax.rsqrt(jnp.mean(widened * widened, axis=-1, keepdims=True) + norm_eps)
    return (normed * gain_row * (1.0 + scale_row) + shift_row).astype(jnp.bfloat16)


def shards(
    latents,
    context,
    condition,
    context_condition,
    norm_gain,
    shift_weight,
    scale_weight,
    gate_weight,
    query_weight,
    key_weight,
    value_weight,
    subtract_share,
    head_gain,
    output_weight,
):
    activated = jax.nn.silu(jnp.stack([condition, context_condition])).astype(jnp.bfloat16)
    partial_terms = jnp.stack(
        [
            jnp.dot(activated, matrix, preferred_element_type=jnp.float32)
            for matrix in (shift_weight, scale_weight, gate_weight)
        ]
    )
    summed = lax.psum(partial_terms, "sp")
    full_terms = lax.all_gather(summed, "tp", axis=2, tiled=True)
    shift_terms, scale_terms, gate_terms = (full_terms[0], full_terms[1], full_terms[2])
    pair_weight = jnp.concatenate([key_weight, value_weight], axis=1)
    joined = jnp.concatenate([query_weight, pair_weight], axis=1)
    projected = jnp.dot(
        modulate(
            lax.all_gather(latents, "tp", axis=0, tiled=True),
            norm_gain,
            shift_terms[0],
            scale_terms[0],
        ),
        joined,
        preferred_element_type=jnp.float32,
    )
    local_count = projected.shape[0]
    positions = lax.axis_index("sp") * local_count + jnp.arange(local_count, dtype=jnp.int32)
    cosine, sine_table = rotary_tables(positions)
    queries = rotate(projected[:, :VALUE].reshape(local_count, 2, HEAD), cosine, sine_table)
    queries = queries.reshape(local_count, VALUE).astype(jnp.bfloat16)
    latent_keys = rotate(
        projected[:, VALUE : 2 * VALUE].reshape(local_count, 2, HEAD), cosine, sine_table
    )
    latent_keys = latent_keys.reshape(local_count, VALUE).astype(jnp.bfloat16)
    latent_pairs = jnp.concatenate(
        [latent_keys, projected[:, 2 * VALUE :].astype(jnp.bfloat16)], axis=1
    )
    context_mod = modulate(context, norm_gain, shift_terms[1], scale_terms[1])
    context_pairs = jnp.dot(context_mod, pair_weight, preferred_element_type=jnp.float32).astype(
        jnp.bfloat16
    )
    sent_pairs = jnp.concatenate([latent_pairs, context_pairs], axis=0)
    arrived = lax.all_gather(sent_pairs, "sp", axis=0, tiled=True)
    updated_carry = []
    for which_map in range(2):
        offset = which_map * HEAD
        scores = jnp.einsum(
            "qd,kd->qk",
            queries[:, offset : offset + HEAD],
            arrived[:, offset : offset + HEAD],
            preferred_element_type=jnp.float32,
        ) * HEAD ** (-0.5)
        powers = jnp.exp(scores)
        updated_carry.append(
            jnp.dot(
                powers.astype(jnp.bfloat16), arrived[:, VALUE:], preferred_element_type=jnp.float32
            )
        )
        updated_carry.append(jnp.sum(powers, axis=1, keepdims=True))
    first_sum, first_total, second_sum, second_total = tuple(updated_carry)
    share_value = subtract_share[0]
    difference = first_sum / first_total - share_value * (second_sum / second_total)
    normed = difference * lax.rsqrt(
        jnp.mean(difference * difference, axis=1, keepdims=True) + head_eps
    )
    head_output = (normed * head_gain * head_scale).astype(jnp.bfloat16)
    branch = lax.psum_scatter(
        jnp.dot(head_output, output_weight, preferred_element_type=jnp.float32),
        "tp",
        scatter_dimension=0,
        tiled=True,
    )
    return (latents.astype(jnp.float32) + gate_terms[0] * branch).astype(jnp.bfloat16)


def solution(mesh):
    in_specs = (
        P(("sp", "tp"), None),
        P("sp", None),
        P("sp"),
        P("sp"),
        P(),
        P("sp", "tp"),
        P("sp", "tp"),
        P("sp", "tp"),
        P(None, "tp"),
        P(None, "tp"),
        P(None, "tp"),
        P("tp"),
        P(),
        P("tp", None),
    )
    out_specs = P(("sp", "tp"), None)
    return jax.shard_map(shards, mesh=mesh, in_specs=in_specs, out_specs=out_specs, check_vma=False)
```

profile of v0, /device:TPU:0, one launch (start us, length us, event | category | flops | bytes accessed | tf_op | source)
XLA Modules:
  0.0 143.5 jit_solution(7154837675321998949)
XLA Ops:
  6.5 0.0 all-gather.2.cloned.1.call-start
  6.6 0.7 all-gather.2.cloned.1.call-update
  7.3 0.0 reduce-scatter.2.cloned.1.call-start
  8.0 0.1 broadcast_multiply_fusion.1
  8.1 0.1 fusion.46
  8.2 0.1 copy.15
  8.4 0.1 copy.18
  8.5 1.1 convolution_bitcast_fusion.1
  9.6 1.1 convolution_bitcast_fusion
  10.7 1.2 convolution_bitcast_fusion.2
  11.9 8.5 %psum.7 = f32[3,2,256]{2,1,0:T(2,128)S(1)} all-reduce(f32[3,2,256]{2,1,0:T(2,128)S(1)} %pad_maximum_fusion.4), channel_id=1, replica_groups=mesh['sp'=4,'tp'=8] {'sp'}, use_global_device_ids=true, to_apply=%region_0.1 | all-reduce | flops 1536 | bytes 12288 | tf_op jit(solution)/shard_map/psum | solution.py:62
  20.4 26.4 %all_gather.9 = f32[3,2,2048]{2,1,0:T(2,128)S(1)} all-gather(f32[3,2,256]{2,1,0:T(2,128)S(1)} %psum.7), channel_id=1, replica_groups=mesh['sp'=4,'tp'=8] {'tp'}, dimensions={2}, use_global_device_ids=true | all-gather | bytes 55296 | tf_op jit(solution)/shard_map/all_gather | solution.py:63
  46.9 0.2 fusion.25
  47.1 0.3 convolution_convert_fusion
  47.5 5.4 %all-gather.2.cloned.1.call-done = bf16[256,2048]{1,0:T(8,128)(2,1)} async-done(((bf16[32,2048]{1,0:T(8,128)(2,1)}), bf16[256,2048]{1,0:T(8,128)(2,1)}) %all-gather.2.cloned.1.call-update) | async-done | bytes 1048592 | tf_op jit(solution)/shard_map/all_gather | solution.py:69
  52.9 1.5 %fusion.2 = f32[256]{0:T(256)S(1)} fusion(bf16[256,2048]{1,0:T(8,128)(2,1)} %all-gather.2.cloned.1.call-done), kind=kLoop, calls=%fused_computation.6 | loop fusion | flops 1572608 | bytes 1049600 | tf_op jit(solution)/shard_map/reduce_sum | solution.py:35
  54.4 2.0 %fusion.7 = f32[256,384]{1,0:T(8,128)S(1)} fusion(bf16[2048,128]{1,0:T(8,128)(2,1)S(1)} %copy-done.4, bf16[2048,128]{1,0:T(8,128)(2,1)S(1)} %copy-done.5, bf16[2048,128]{1,0:T(8,128)(2,1)S(1)} %copy-done.6, bf16[256,2048]{1,0:T(8,128)(2,1)} %all-gather.2.cloned.1.call-done, f32[2048]{0:T(1024)S(1)} %bitcast.40, f32[2048]{0:T(1024)S(1)} %bitcast.41, ...), kind=kOutput, calls=%fused_computation.11 | convolution fusion | flops 410517504 | bytes 3040256 | tf_op jit(solution)/shard_map/dot_general | solution.py:67
  56.5 0.1 copy.16
  56.6 0.1 copy.17
  56.7 0.1 copy.20
  56.8 0.1 copy.21
  57.0 7.9 %all_gather.11 = bf16[1280,256]{1,0:T(8,128)(2,1)S(1)} all-gather(bf16[320,256]{1,0:T(8,128)(2,1)S(1)} %pad_maximum_fusion), channel_id=1, replica_groups=mesh['sp'=4,'tp'=8] {'sp'}, dimensions={0}, use_global_device_ids=true | all-gather | bytes 819200 | tf_op jit(solution)/shard_map/all_gather | solution.py:94
  64.9 0.5 fusion.59
  65.4 0.0 copy-start.3
  65.5 0.5 fusion.60
  65.9 0.4 fusion.14
  66.3 0.4 multiply_reduce_fusion
  66.7 0.0 copy-start.1
  66.8 1.9 %fusion.39 = f32[256,2048]{1,0:T(8,128)} fusion(bf16[128,2048]{1,0:T(8,128)(2,1)S(1)} %copy-done, f32[256,128]{0,1:T(8,128)S(1)} %get-tuple-element.27, f32[128]{0:T(128)S(1)} %copy-done.3, f32[256]{0:T(256)S(1)} %add_rsqrt_fusion), kind=kOutput, calls=%fused_computation.58 | convolution fusion | flops 134348800 | bytes 2754048 | tf_op jit(solution)/shard_map/dot_general | solution.py:119
  68.6 0.0 reduce-scatter.2.cloned.1.call-update
  68.6 66.4 %reduce-scatter.2.cloned.1.call-done = f32[32,2048]{1,0:T(8,128)} async-done(((f32[256,2048]{1,0:T(8,128)}), f32[32,2048]{1,0:T(8,128)}) %reduce-scatter.2.cloned.1.call-update) | async-done | bytes 262160 | tf_op jit(solution)/shard_map/reduce_scatter | solution.py:118
  135.0 1.6 %add_convert_fusion = bf16[32,2048]{1,0:T(8,128)(2,1)} fusion(f32[32,2048]{1,0:T(8,128)} %reduce-scatter.2.cloned.1.call-done, bf16[32,2048]{1,0:T(8,128)(2,1)S(1)} %copy-done.1, f32[2048]{0:T(1024)S(1)} %bitcast.33), kind=kLoop, calls=%fused_computation.45 | loop fusion | flops 262144 | bytes 532480 | tf_op jit(solution)/shard_map/convert_element_type | solution.py:124
  (31 shorter events, 0.3 us)
Async XLA Ops:
  6.5 60.2 %copy-start = (bf16[128,2048]{1,0:T(8,128)(2,1)S(1)}, bf16[128,2048]{1,0:T(8,128)(2,1)}, u32[]{:S(2)}) copy-start(bf16[128,2048]{1,0:T(8,128)(2,1)} %param.27) | copy-start | bytes 1572868
  6.5 40.4 %copy-start.2 = (bf16[64,2048]{1,0:T(8,128)(2,1)S(1)}, bf16[64,2048]{1,0:T(8,128)(2,1)}, u32[]{:S(2)}) copy-start(bf16[64,2048]{1,0:T(8,128)(2,1)} %param.15) | copy-start | bytes 786436
  6.5 40.6 %copy-start.4 = (bf16[2048,128]{1,0:T(8,128)(2,1)S(1)}, bf16[2048,128]{1,0:T(8,128)(2,1)}, u32[]{:S(2)}) copy-start(bf16[2048,128]{1,0:T(8,128)(2,1)} %param.24) | copy-start | bytes 1572868
  6.5 40.6 %copy-start.5 = (bf16[2048,128]{1,0:T(8,128)(2,1)S(1)}, bf16[2048,128]{1,0:T(8,128)(2,1)}, u32[]{:S(2)}) copy-start(bf16[2048,128]{1,0:T(8,128)(2,1)} %param.23) | copy-start | bytes 1572868
  6.5 40.6 %copy-start.7 = (f32[2048]{0:T(1024)S(1)}, f32[2048]{0:T(1024)}, u32[]{:S(2)}) copy-start(f32[2048]{0:T(1024)} %param.18) | copy-start | bytes 24580
  6.5 46.3 %all-gather.2.cloned.1.call-start = ((), (), s32[]{:S(2)}) async-start(), calls=%async_computation.1 | async-start | bytes 1179648 | tf_op jit(solution)/shard_map/all_gather | solution.py:69
  7.3 127.7 %reduce-scatter.2.cloned.1.call-start = ((), (), s32[]{:S(2)}) async-start(), calls=%async_computation.2 | async-start | bytes 2359296 | tf_op jit(solution)/shard_map/reduce_scatter | solution.py:118
  10.7 43.7 %copy-start.6 = (bf16[2048,128]{1,0:T(8,128)(2,1)S(1)}, bf16[2048,128]{1,0:T(8,128)(2,1)}, u32[]{:S(2)}) copy-start(bf16[2048,128]{1,0:T(8,128)(2,1)} %param.22) | copy-start | bytes 1572868
  65.4 1.3 copy-start.3
  66.7 68.3 %copy-start.1 = (bf16[32,2048]{1,0:T(8,128)(2,1)S(1)}, bf16[32,2048]{1,0:T(8,128)(2,1)}, u32[]{:S(2)}) copy-start(bf16[32,2048]{1,0:T(8,128)(2,1)} %param.14) | copy-start | bytes 393220
Sparse Core Ops, SparseCore 0:
  9.5 43.3 all-gather.1
  68.8 66.2 reduce-scatter.1
where the time goes:
time: 144 us; the launch traced here: 143 us
  waiting for transfers between devices  72.5 us (50%)
  blocking collectives  42.9 us (30%)
  between operations  14.3 us (10%)
  matrix products  9.42 us (7%)
  other arithmetic  3.7 us (3%)
    reduce_scatter x1, waiting for transfers between devices, shards(): lax.psum_scatter(jnp.dot(head_output, output_weight, preferred_element_ty...  66.4 us
    all_gather x1, blocking collectives, shards(): full_terms = lax.all_gather(summed, 'tp', axis=2, tiled=True)  26.4 us
    psum x1, blocking collectives, shards(): summed = lax.psum(partial_terms, 'sp')  8.51 us
    all_gather x1, blocking collectives, shards(): arrived = lax.all_gather(sent_pairs, 'sp', axis=0, tiled=True)  7.9 us
    all_gather x1, waiting for transfers between devices, shards(): lax.all_gather(latents, 'tp', axis=0, tiled=True)  5.4 us
    dot_general x3, matrix products, shards(): jnp.dot(activated, matrix, preferred_element_type=jnp.float32)  3.45 us
  transfers between devices with their start and end apart: 2, of which 2 were waited for; matrix products, arithmetic and copies ran while one was open for 3% of the time, Pallas kernels for 0%

commit v1 on v0

--- a/solution.py
+++ b/solution.py
@@ -91,7 +91,17 @@
         jnp.bfloat16
     )
     sent_pairs = jnp.concatenate([latent_pairs, context_pairs], axis=0)
-    arrived = lax.all_gather(sent_pairs, "sp", axis=0, tiled=True)
+    devs = lax.axis_size("sp")
+    cards = [sent_pairs]
+    dev_i = 0
+    while dev_i < devs - 1:
+        cards.append(lax.ppermute(cards[-1], "sp", [(c, (c + 1) % devs) for c in range(devs)]))
+        dev_i = dev_i + 1
+    arrived = jnp.roll(
+        jnp.concatenate(cards[::-1], axis=0),
+        shift=(lax.axis_index("sp") + 1) * sent_pairs.shape[0],
+        axis=0,
+    )
     updated_carry = []
     for which_map in range(2):
         offset = which_map * HEAD

time: 144 us -> 151 us (1.049)
  waiting for transfers between devices: 72.5 us -> 89.1 us
  blocking collectives: 42.9 us -> 35.2 us
  matrix products: 9.42 us -> 7.83 us
    ppermute x0 -> x3, waiting for transfers between devices: none -> 13.6 us  [shards(): lax.ppermute(cards[-1], 'sp', [(c, (c + 1) % devs) for c in range(devs)])]
    all_gather x1 -> x0, blocking collectives: 7.9 us -> none  [shards(): arrived = lax.all_gather(sent_pairs, 'sp', axis=0, tiled=True)]
    all_gather x1, waiting for transfers between devices: 5.4 us -> 7.8 us  [shards(): lax.all_gather(latents, 'tp', axis=0, tiled=True)]
    dot_general x3, matrix products: 3.45 us -> 1.43 us  [shards(): jnp.dot(activated, matrix, preferred_element_type=jnp.float32)]
  transfers between devices with their start and end apart: 2 -> 5, of which waited for: 2 -> 5; matrix products, arithmetic and copies ran while one was open for 3% -> 2% of each run, Pallas kernels for 0% -> 0%
where the time goes in v1:
time: 151 us
  waiting for transfers between devices  89.1 us (59%)
  blocking collectives  35.2 us (23%)
  between operations  14.5 us (10%)
  matrix products  7.83 us (5%)
  other arithmetic  3.75 us (2%)
    reduce_scatter x1, waiting for transfers between devices, shards(): lax.psum_scatter(jnp.dot(head_output, output_weight, preferred_element_ty...  67 us
    all_gather x1, blocking collectives, shards(): full_terms = lax.all_gather(summed, 'tp', axis=2, tiled=True)  26.7 us
    ppermute x3, waiting for transfers between devices, shards(): lax.ppermute(cards[-1], 'sp', [(c, (c + 1) % devs) for c in range(devs)])  13.6 us
    psum x1, blocking collectives, shards(): summed = lax.psum(partial_terms, 'sp')  8.5 us
    all_gather x1, waiting for transfers between devices, shards(): lax.all_gather(latents, 'tp', axis=0, tiled=True)  7.8 us
  transfers between devices with their start and end apart: 5, of which 5 were waited for; matrix products, arithmetic and copies ran while one was open for 2% of the time, Pallas kernels for 0%

profile of v1, /device:TPU:0, one launch (start us, length us, event | category | flops | bytes accessed | tf_op | source)
XLA Modules:
  0.0 151.2 jit_solution(8445394811532671346)
XLA Ops:
  6.6 0.0 all-gather.2.cloned.1.call-start
  6.6 0.7 all-gather.2.cloned.1.call-update
  7.3 0.0 reduce-scatter.2.cloned.1.call-start
  7.4 0.1 broadcast_multiply_fusion.1
  7.5 0.1 fusion.48
  7.6 0.1 copy.15
  7.8 0.1 copy.18
  7.9 1.1 convolution_bitcast_fusion
  9.0 0.1 convolution_bitcast_fusion.1
  9.2 0.1 convolution_bitcast_fusion.2
  9.3 8.5 %psum.7 = f32[3,2,256]{2,1,0:T(2,128)S(1)} all-reduce(f32[3,2,256]{2,1,0:T(2,128)S(1)} %pad_maximum_fusion.5), channel_id=1, replica_groups=mesh['sp'=4,'tp'=8] {'sp'}, use_global_device_ids=true, to_apply=%region_0.1 | all-reduce | flops 1536 | bytes 12288 | tf_op jit(solution)/shard_map/psum | solution.py:62
  17.8 26.7 %all_gather.6 = f32[3,2,2048]{2,1,0:T(2,128)S(1)} all-gather(f32[3,2,256]{2,1,0:T(2,128)S(1)} %psum.7), channel_id=1, replica_groups=mesh['sp'=4,'tp'=8] {'tp'}, dimensions={2}, use_global_device_ids=true | all-gather | bytes 55296 | tf_op jit(solution)/shard_map/all_gather | solution.py:63
  44.5 0.2 fusion.25
  44.8 0.3 convolution_convert_fusion
  45.1 7.8 %all-gather.2.cloned.1.call-done = bf16[256,2048]{1,0:T(8,128)(2,1)} async-done(((bf16[32,2048]{1,0:T(8,128)(2,1)}), bf16[256,2048]{1,0:T(8,128)(2,1)}) %all-gather.2.cloned.1.call-update) | async-done | bytes 1048592 | tf_op jit(solution)/shard_map/all_gather | solution.py:69
  52.9 1.5 fusion.2
  54.4 2.0 %fusion.7 = f32[256,384]{1,0:T(8,128)S(1)} fusion(bf16[2048,128]{1,0:T(8,128)(2,1)S(1)} %copy-done.8, bf16[2048,128]{1,0:T(8,128)(2,1)S(1)} %copy-done.9, bf16[2048,128]{1,0:T(8,128)(2,1)S(1)} %copy-done.10, bf16[256,2048]{1,0:T(8,128)(2,1)} %all-gather.2.cloned.1.call-done, f32[2048]{0:T(1024)S(1)} %bitcast.40, f32[2048]{0:T(1024)S(1)} %bitcast.41, ...), kind=kOutput, calls=%fused_computation.11 | convolution fusion | flops 410517504 | bytes 3040256 | tf_op jit(solution)/shard_map/dot_general | solution.py:67
  56.5 0.1 copy.20
  56.7 0.1 copy.21
  56.8 0.1 copy.16
  56.9 0.1 copy.17
  57.1 0.1 collective-permute-start
  57.1 4.7 %collective-permute-done = bf16[320,256]{1,0:T(8,128)(2,1)S(1)} collective-permute-done((bf16[320,256]{1,0:T(8,128)(2,1)S(1)}, bf16[320,256]{1,0:T(8,128)(2,1)S(1)}, u32[]{:S(2)}, u32[]{:S(2)}) %collective-permute-start) | collective-permute-done | bytes 163872 | tf_op jit(solution)/shard_map/ppermute | solution.py:98
  61.9 4.7 %collective-permute-done.1 = bf16[320,256]{1,0:T(8,128)(2,1)S(1)} collective-permute-done((bf16[320,256]{1,0:T(8,128)(2,1)S(1)}, bf16[320,256]{1,0:T(8,128)(2,1)S(1)}, u32[]{:S(2)}, u32[]{:S(2)}) %collective-permute-start.1) | collective-permute-done | bytes 163872 | tf_op jit(solution)/shard_map/ppermute | solution.py:98
  67.3 4.1 %collective-permute-done.2 = bf16[320,256]{1,0:T(8,128)(2,1)S(1)} collective-permute-done((bf16[320,256]{1,0:T(8,128)(2,1)S(1)}, bf16[320,256]{1,0:T(8,128)(2,1)S(1)}, u32[]{:S(2)}, u32[]{:S(2)}) %collective-permute-start.2) | collective-permute-done | bytes 163872 | tf_op jit(solution)/shard_map/ppermute | solution.py:98
  71.6 0.5 fusion.63
  72.0 0.5 fusion.62
  72.6 0.5 fusion.14
  73.1 0.6 multiply_reduce_fusion
  73.8 1.9 %fusion.41 = f32[256,2048]{1,0:T(8,128)} fusion(bf16[128,2048]{1,0:T(8,128)(2,1)S(1)} %copy-done, f32[256,128]{0,1:T(8,128)S(1)} %get-tuple-element.27, f32[128]{0:T(128)S(1)} %copy-done.7, f32[256]{0:T(256)S(1)} %add_rsqrt_fusion), kind=kOutput, calls=%fused_computation.61 | convolution fusion | flops 134348800 | bytes 2754048 | tf_op jit(solution)/shard_map/dot_general | solution.py:129
  75.7 67.0 %reduce-scatter.2.cloned.1.call-done = f32[32,2048]{1,0:T(8,128)} async-done(((f32[256,2048]{1,0:T(8,128)}), f32[32,2048]{1,0:T(8,128)}) %reduce-scatter.2.cloned.1.call-update) | async-done | bytes 262160 | tf_op jit(solution)/shard_map/reduce_scatter | solution.py:128
  142.7 1.6 %add_convert_fusion = bf16[32,2048]{1,0:T(8,128)(2,1)} fusion(f32[32,2048]{1,0:T(8,128)} %reduce-scatter.2.cloned.1.call-done, bf16[32,2048]{1,0:T(8,128)(2,1)S(1)} %copy-done.1, f32[2048]{0:T(1024)S(1)} %bitcast.33), kind=kLoop, calls=%fused_computation.45 | loop fusion | flops 262144 | bytes 532480 | tf_op jit(solution)/shard_map/convert_element_type | solution.py:134
  (54 shorter events, 0.4 us)
Async XLA Ops:
  6.5 67.2 %copy-start = (bf16[128,2048]{1,0:T(8,128)(2,1)S(1)}, bf16[128,2048]{1,0:T(8,128)(2,1)}, u32[]{:S(2)}) copy-start(bf16[128,2048]{1,0:T(8,128)(2,1)} %param.27) | copy-start | bytes 1572868
  6.5 2.5 %copy-start.6 = (f32[512]{0:T(512)S(1)}, f32[512]{0:T(512)}, u32[]{:S(2)}) copy-start(f32[512]{0:T(512)} %param.16) | copy-start | bytes 6148
  6.5 2.5 %copy-start.5 = (f32[512]{0:T(512)S(1)}, f32[512]{0:T(512)}, u32[]{:S(2)}) copy-start(f32[512]{0:T(512)} %param.17) | copy-start | bytes 6148
  6.5 2.5 %copy-start.2 = (bf16[512,256]{1,0:T(8,128)(2,1)S(1)}, bf16[512,256]{1,0:T(8,128)(2,1)}, u32[]{:S(2)}) copy-start(bf16[512,256]{1,0:T(8,128)(2,1)} %param.20) | copy-start | bytes 786436
  6.5 2.6 %copy-start.3 = (bf16[512,256]{1,0:T(8,128)(2,1)S(1)}, bf16[512,256]{1,0:T(8,128)(2,1)}, u32[]{:S(2)}) copy-start(bf16[512,256]{1,0:T(8,128)(2,1)} %param.19) | copy-start | bytes 786436
  6.5 38.0 %copy-start.4 = (bf16[64,2048]{1,0:T(8,128)(2,1)S(1)}, bf16[64,2048]{1,0:T(8,128)(2,1)}, u32[]{:S(2)}) copy-start(bf16[64,2048]{1,0:T(8,128)(2,1)} %param.15) | copy-start | bytes 786436
  6.6 38.2 %copy-start.11 = (f32[2048]{0:T(1024)S(1)}, f32[2048]{0:T(1024)}, u32[]{:S(2)}) copy-start(f32[2048]{0:T(1024)} %param.18) | copy-start | bytes 24580
  6.6 38.2 %copy-start.9 = (bf16[2048,128]{1,0:T(8,128)(2,1)S(1)}, bf16[2048,128]{1,0:T(8,128)(2,1)}, u32[]{:S(2)}) copy-start(bf16[2048,128]{1,0:T(8,128)(2,1)} %param.23) | copy-start | bytes 1572868
  6.6 38.2 %copy-start.8 = (bf16[2048,128]{1,0:T(8,128)(2,1)S(1)}, bf16[2048,128]{1,0:T(8,128)(2,1)}, u32[]{:S(2)}) copy-start(bf16[2048,128]{1,0:T(8,128)(2,1)} %param.24) | copy-start | bytes 1572868
  6.6 46.3 %all-gather.2.cloned.1.call-start = ((), (), s32[]{:S(2)}) async-start(), calls=%async_computation.1 | async-start | bytes 1179648 | tf_op jit(solution)/shard_map/all_gather | solution.py:69
  7.3 135.3 %reduce-scatter.2.cloned.1.call-start = ((), (), s32[]{:S(2)}) async-start(), calls=%async_computation.2 | async-start | bytes 2359296 | tf_op jit(solution)/shard_map/reduce_scatter | solution.py:128
  44.7 9.7 %copy-start.10 = (bf16[2048,128]{1,0:T(8,128)(2,1)S(1)}, bf16[2048,128]{1,0:T(8,128)(2,1)}, u32[]{:S(2)}) copy-start(bf16[2048,128]{1,0:T(8,128)(2,1)} %param.22) | copy-start | bytes 1572868
  57.1 4.8 %collective-permute-start = (bf16[320,256]{1,0:T(8,128)(2,1)S(1)}, bf16[320,256]{1,0:T(8,128)(2,1)S(1)}, u32[]{:S(2)}, u32[]{:S(2)}) collective-permute-start(bf16[320,256]{1,0:T(8,128)(2,1)S(1)} %pad_maximum_fusion), channel_id=1, source_target_pairs={{0,8},{8,16},{16,24},{24,0},{1,9},{9,17},{17,25},{25,1},{2,10},{10... | collective-permute-start | bytes 491528 | tf_op jit(solution)/shard_map/ppermute | solution.py:98
  61.9 4.7 %collective-permute-start.1 = (bf16[320,256]{1,0:T(8,128)(2,1)S(1)}, bf16[320,256]{1,0:T(8,128)(2,1)S(1)}, u32[]{:S(2)}, u32[]{:S(2)}) collective-permute-start(bf16[320,256]{1,0:T(8,128)(2,1)S(1)} %collective-permute-done), channel_id=1, source_target_pairs={{0,8},{8,16},{16,24},{24,0},{1,9},{9,17},{17,25},{25,1},{2,10},{10... | collective-permute-start | bytes 491528 | tf_op jit(solution)/shard_map/ppermute | solution.py:98
  66.6 4.7 %collective-permute-start.2 = (bf16[320,256]{1,0:T(8,128)(2,1)S(1)}, bf16[320,256]{1,0:T(8,128)(2,1)S(1)}, u32[]{:S(2)}, u32[]{:S(2)}) collective-permute-start(bf16[320,256]{1,0:T(8,128)(2,1)S(1)} %collective-permute-done.1), channel_id=1, source_target_pairs={{0,8},{8,16},{16,24},{24,0},{1,9},{9,17},{17,25},{25,1},{2,10},{10... | collective-permute-start | bytes 491528 | tf_op jit(solution)/shard_map/ppermute | solution.py:98
  72.5 1.2 copy-start.7
  75.6 67.0 %copy-start.1 = (bf16[32,2048]{1,0:T(8,128)(2,1)S(1)}, bf16[32,2048]{1,0:T(8,128)(2,1)}, u32[]{:S(2)}) copy-start(bf16[32,2048]{1,0:T(8,128)(2,1)} %param.14) | copy-start | bytes 393220
Sparse Core Ops, SparseCore 0:
  9.5 43.3 all-gather.1
  75.8 66.8 reduce-scatter.1
